TPU v7x, 512 devices: a whole 4x8x8 slice. The times are simulated.
512 devices in a mesh: sp: 32 (over z, x), tp: 16 (over y, core).
Axes of the slice: x: 4, y: 8, z: 8, core: 2. Of those that a mesh axis runs over, the one named last changes fastest.
Arguments:
- hidden_in: bfloat16 [2, 49152, 2048], P(None, ('sp', 'tp')), may hold values from -6 to 6
- w_value: bfloat16 [2048, 2048], P(None, 'tp'), may hold values from -0.125 to 0.125
- w_key: bfloat16 [2048, 2048], P(None, 'tp'), may hold values from -0.125 to 0.125
- w_step: bfloat16 [2048, 32], replicated, may hold values from -0.125 to 0.125
- conv_value: bfloat16 [4, 2048], P(None, 'tp'), may hold values from -3 to 3
- conv_key: bfloat16 [4, 2048], P(None, 'tp'), may hold values from -3 to 3
- step_bias: float32 [32], P('tp'), may hold values from -3 to -1
- decay_rate: float32 [32], P('tp'), may hold values from 2.03450521e-06 to 0.25
- decay_jump: float32 [2, 49152, 32], P(None, 'sp', 'tp'), may hold values from -0.75 to 0
- new_value: bfloat16 [2, 2048], P(None, 'tp'), may hold values from -60 to 60
- new_key: bfloat16 [2, 2048], P(None, 'tp'), may hold values from -6 to 6
- new_query: bfloat16 [2, 2048], P(None, 'tp'), may hold values from -6 to 6
- new_gate: bfloat16 [2, 2048], P(None, 'tp'), may hold values from -6 to 6
- new_step: float32 [2, 32], P(None, 'tp'), may hold values from -6 to 6
- read_gain: bfloat16 [2048], P('tp'), may hold values from 0.099609375 to 1.8984375
Outputs:
- prompt_state: bfloat16 [2, 32, 64, 128], P(None, 'tp', 'sp')
- read_out: bfloat16 [2, 32, 64], P(None, 'tp', 'sp')
All inputs are finite; a program needn't handle non-finite values.
Results may differ from a plain program's by a relative error of at most 0.006.
Values may be sent and summed in bfloat16 or wider, within the bound.
No kernel may reach another device: no remote copies, remote signals or barrier semaphores. Data moves between devices by JAX's collectives and lax.ppermute only.
A program may use at most 64 MiB of HBM per device.

v0:
```python
import jax
import jax.numpy as jnp
from jax import lax
from jax.sharding import PartitionSpec as P

HEAD_DIM = 64
STATE = 128
EPSILON = 1e-05


def shifted(value, axis, steps):
    count = lax.axis_size(axis)
    leading, last = (max(0, -steps), min(count, count - steps))
    return lax.ppermute(value, axis, [(source, source + steps) for source in range(leading, last)])


def sent_to_all(shard, axis):
    length = lax.axis_size(axis)
    return lax.all_to_all(
        jnp.broadcast_to(shard[None], (length, *shard.shape)), axis, 0, 0, tiled=True
    )


def taken_together(shard, axis):
    everything = sent_to_all(shard, axis)
    return jnp.sum(everything, axis=0)


def causal_mix(padded_rows, conv_taps):
    tap_count = conv_taps.shape[0]
    length = padded_rows.shape[-2] - tap_count + 1
    running = jnp.zeros(padded_rows.shape[:-2] + (length, padded_rows.shape[-1]), jnp.float32)
    for tap_index in range(tap_count):
        running = running + padded_rows[..., tap_index : tap_index + length, :].astype(
            jnp.float32
        ) * conv_taps[tap_index].astype(jnp.float32)
    return running


def block_states(mixed_rows, weight, value_cols, groups_dev):
    seq_count, row_count, heads_dev = weight.shape
    per_group = heads_dev // groups_dev
    values = (
        mixed_rows[:, :, :value_cols].reshape(seq_count, row_count, groups_dev, per_group, HEAD_DIM)
        * weight.reshape(seq_count, row_count, groups_dev, per_group)[..., None]
    )
    keys = mixed_rows[:, :, value_cols:].reshape(seq_count, row_count, groups_dev, STATE)
    states = jnp.einsum("slgep,slgn->sgepn", values, keys, precision=lax.Precision.HIGHEST)
    return states.reshape(seq_count, heads_dev, HEAD_DIM, STATE)


def per_device(
    hidden_in,
    w_value,
    w_key,
    w_step,
    conv_value,
    conv_key,
    step_bias,
    decay_rate,
    decay_jump,
    new_value,
    new_key,
    new_query,
    new_gate,
    new_step,
    read_gain,
):
    sp_count = lax.axis_size("sp")
    sp_index = lax.axis_index("sp")
    tp_index = lax.axis_index("tp")
    heads_dev = step_bias.shape[0]
    value_cols = w_value.shape[1]
    key_cols = w_key.shape[1]
    groups_dev = key_cols // STATE
    per_group = heads_dev // groups_dev
    kernel_taps = conv_value.shape[0]
    seq_count = hidden_in.shape[0]
    share = HEAD_DIM // sp_count
    own_step = lax.dynamic_slice_in_dim(w_step, tp_index * heads_dev, heads_dev, 1)
    w_joined = jnp.concatenate([w_value, w_key, own_step], axis=1)
    projected = jnp.einsum(
        "tfy,yz->tfz",
        lax.all_gather(hidden_in, "tp", axis=1, tiled=True),
        w_joined,
        preferred_element_type=jnp.float32,
    ).astype(jnp.bfloat16)
    seg_rows = projected.shape[1]
    proj_pair = projected[:, :, : value_cols + key_cols]
    proj_step = projected[:, :, value_cols + key_cols :]
    step_size = jax.nn.softplus(proj_step.astype(jnp.float32) + step_bias)
    log_decay = decay_jump - decay_rate * step_size
    conv_taps = jnp.concatenate([conv_value, conv_key], axis=1)
    edge_rows = shifted(proj_pair[:, seg_rows - (kernel_taps - 1) :, :], "sp", 1)
    mixed_rows = jax.nn.silu(causal_mix(jnp.concatenate([edge_rows, proj_pair], axis=1), conv_taps))
    seg_total = jnp.sum(log_decay, axis=1)
    decay_after = seg_total[:, None, :] - jnp.cumsum(log_decay, axis=1)
    seg_states = block_states(mixed_rows, step_size * jnp.exp(decay_after), value_cols, groups_dev)
    tiled_totals = jnp.broadcast_to(
        seg_total[:, None, :, None], (seq_count, 1, heads_dev, sp_count)
    )
    got_states, got_totals = (
        lax.all_to_all(seg_states[:, None], "sp", split_axis=3, concat_axis=1, tiled=True),
        lax.all_to_all(tiled_totals, "sp", split_axis=3, concat_axis=1, tiled=True),
    )
    got_totals = got_totals[..., 0]
    tail_decay = jnp.sum(got_totals, axis=1, keepdims=True) - jnp.cumsum(got_totals, axis=1)
    final_state = jnp.einsum(
        "sjh,sjhpn->shpn", jnp.exp(tail_decay), got_states, precision=lax.Precision.HIGHEST
    )
    cache_state = final_state.astype(jnp.bfloat16)
    new_size = jax.nn.softplus(new_step + step_bias)
    keep_share = jnp.exp(-decay_rate * new_size)
    query = new_query.astype(jnp.float32).reshape(seq_count, groups_dev, STATE)
    own_key = new_key.astype(jnp.float32).reshape(seq_count, groups_dev, STATE)
    key_match = jnp.sum(own_key * query, axis=-1)
    size_grid = new_size.reshape(seq_count, groups_dev, per_group)
    keep_grid = keep_share.reshape(seq_count, groups_dev, per_group)
    value_grid = new_value.astype(jnp.float32).reshape(seq_count, groups_dev, per_group, HEAD_DIM)
    gate_grid = jax.nn.silu(new_gate.astype(jnp.float32)).reshape(
        seq_count, groups_dev, per_group, HEAD_DIM
    )
    gain_grid = read_gain.astype(jnp.float32).reshape(groups_dev, per_group, HEAD_DIM)
    own_value = lax.dynamic_slice_in_dim(value_grid, sp_index * share, share, 3)
    own_gate = lax.dynamic_slice_in_dim(gate_grid, sp_index * share, share, 3)
    own_gain = lax.dynamic_slice_in_dim(gain_grid, sp_index * share, share, 2)
    state_read = jnp.einsum(
        "sgepn,sgn->sgep",
        final_state.reshape(seq_count, groups_dev, per_group, share, STATE),
        query,
        precision=lax.Precision.HIGHEST,
    )
    raw_read = (
        keep_grid[..., None] * state_read
        + size_grid[..., None] * own_value * key_match[:, :, None, None]
    )
    gated = raw_read * own_gate
    squares = taken_together(jnp.sum(gated * gated, axis=(2, 3)), "sp")
    scale = lax.rsqrt(squares / (per_group * HEAD_DIM) + EPSILON)
    read_out = (gated * scale[:, :, None, None] * own_gain).astype(jnp.bfloat16)
    return (cache_state, read_out.reshape(seq_count, heads_dev, share))


def solution(mesh):
    return jax.shard_map(
        per_device,
        mesh=mesh,
        in_specs=(
            P(None, ("sp", "tp"), None),
            P(None, "tp"),
            P(None, "tp"),
            P(),
            P(None, "tp"),
            P(None, "tp"),
            P("tp"),
            P("tp"),
            P(None, "sp", "tp"),
            P(None, "tp"),
            P(None, "tp"),
            P(None, "tp"),
            P(None, "tp"),
            P(None, "tp"),
            P("tp"),
        ),
        out_specs=(P(None, "tp", "sp", None), P(None, "tp", "sp")),
        check_vma=False,
    )
```

profile of v0, /device:TPU:24, one launch (start us, length us, event | category | flops | bytes accessed | tf_op | source)
XLA Modules:
  0.0 168.7 jit_solution(7346045088244292500)
XLA Ops:
  7.2 0.7 all-gather.2.cloned.1.call-update
  7.9 1.2 copy.25
  9.2 1.2 copy.26
  10.4 0.7 neg.21
  11.1 0.7 convert_multiply_fusion
  11.8 0.7 reshape.141
  12.6 0.7 reshape.143
  13.3 0.7 constant_dynamic-update-slice_fusion.1
  14.0 0.7 constant_dynamic-update-slice_fusion
  14.7 0.8 multiply_reduce_fusion.1
  15.5 0.7 multiply_exponential_fusion
  16.3 75.9 %all-gather.2.cloned.1.call-done = bf16[2,1536,2048]{2,1,0:T(8,128)(2,1)} async-done(((bf16[2,96,2048]{2,1,0:T(8,128)(2,1)}), bf16[2,1536,2048]{2,1,0:T(8,128)(2,1)}) %all-gather.2.cloned.1.call-update) | async-done | bytes 12582928 | tf_op jit(solution)/shard_map/all_gather | solution.py:84
  92.2 8.1 %fusion = bf16[2,1536,258]{1,2,0:T(8,128)(2,1)S(1)} fusion(bf16[2,1536,2048]{2,1,0:T(8,128)(2,1)} %all-gather.2.cloned.1.call-done, bf16[2048,2]{0,1:T(2,128)(2,1)S(1)} %constant_dynamic-slice_fusion, bf16[2048,128]{0,1:T(8,128)(2,1)S(1)} %copy.26, bf16[2048,128]{0,1:T(8,128)(2,1)S(1)} %copy.25), kind=kOutput, calls=%fused_computation.2 | convolution fusion | flops 3250354176 | bytes 15224832 | tf_op jit(solution)/shard_map/tfy,yz->tfz/dot_general | solution.py:82
  100.3 0.7 slice.58
  101.1 0.2 fusion.23
  101.3 1.2 reduce-window.6
  102.7 0.4 reduce-window.9
  103.1 3.4 %collective-permute-start = (bf16[2,3,256]{1,2,0:T(8,128)(2,1)}, bf16[2,3,256]{1,2,0:T(8,128)(2,1)S(1)}, u32[]{:S(2)}, u32[]{:S(2)}) collective-permute-start(bf16[2,3,256]{1,2,0:T(8,128)(2,1)} %slice.58), channel_id=1, source_target_pairs={{0,16},{16,32},{32,48},{48,64},{64,80},{80,96},{96,112},{112,128},... | collective-permute-start | bytes 9224 | tf_op jit(solution)/shard_map/ppermute | solution.py:14
  106.5 0.6 broadcast_in_dim.4
  107.1 9.9 %all-to-all-start = ((f32[2,1,2,32]{2,0,1,3:T(2,128)}), f32[2,1,2,32]{2,0,1,3:T(2,128)S(1)}, u32[]{:S(2)}, u32[]{:S(2)}) async-start(f32[2,1,2,32]{2,0,1,3:T(2,128)} %broadcast_in_dim.4), calls=%async_computation | async-start | bytes 65536 | tf_op jit(solution)/shard_map/all_to_all | solution.py:104
  117.3 9.5 %all-to-all-done = f32[2,1,2,32]{2,0,1,3:T(2,128)S(1)} async-done(((f32[2,1,2,32]{2,0,1,3:T(2,128)}), f32[2,1,2,32]{2,0,1,3:T(2,128)S(1)}, u32[]{:S(2)}, u32[]{:S(2)}) %all-to-all-start) | async-done | bytes 544 | tf_op jit(solution)/shard_map/all_to_all | solution.py:104
  126.9 2.6 %divide_multiply_fusion = f32[2,1536,256]{1,2,0:T(8,128)S(1)} fusion(bf16[2,1536,256]{1,2,0:T(8,128)(2,1)S(1)} %slice.59, bf16[2,3,256]{1,2,0:T(8,128)(2,1)S(1)} %collective-permute-done, f32[256]{0:T(256)S(1)} %bitcast.61, f32[256]{0:T(256)S(1)} %bitcast.62, f32[256]{0:T(256)S(1)} %bitcast.63, f32[256]{0:T(256)S(1)} %bitcast.60), kind=kLoop, calls=%fused_computation | loop fusion | flops 18874368 | bytes 4725760 | tf_op jit(solution)/shard_map/jit(silu)/mul | solution.py:95
  129.7 1.7 fusion.5
  131.3 0.7 copy.30
  132.1 3.9 %all-to-all-start.1 = ((f32[2,1,2,64,128]{4,2,0,1,3:T(2,128)}), f32[2,1,2,64,128]{4,2,0,1,3:T(2,128)S(1)}, u32[]{:S(2)}, u32[]{:S(2)}) async-start(f32[2,1,2,64,128]{4,2,0,1,3:T(2,128)} %copy.30), calls=%async_computation.1 | async-start | bytes 262144 | tf_op jit(solution)/shard_map/all_to_all | solution.py:103
  136.2 10.3 %all-to-all-done.1 = f32[2,1,2,64,128]{4,2,0,1,3:T(2,128)S(1)} async-done(((f32[2,1,2,64,128]{4,2,0,1,3:T(2,128)}), f32[2,1,2,64,128]{4,2,0,1,3:T(2,128)S(1)}, u32[]{:S(2)}, u32[]{:S(2)}) %all-to-all-start.1) | async-done | bytes 131104 | tf_op jit(solution)/shard_map/all_to_all | solution.py:103
  146.6 0.2 fusion.19
  147.0 0.6 broadcast_in_dim.5
  147.7 3.9 %all-to-all-start.2 = ((f32[32,2,1]{1,2,0:T(1,128)}), f32[32,2,1]{1,2,0:T(1,128)S(1)}, u32[]{:S(2)}, u32[]{:S(2)}) async-start(f32[32,2,1]{1,2,0:T(1,128)} %broadcast_in_dim.5), calls=%async_computation.2 | async-start | bytes 32768 | tf_op jit(solution)/shard_map/all_to_all | solution.py:19
  151.6 0.6 convert_element_type.93
  152.2 8.9 %all-to-all-done.2 = f32[32,2,1]{1,2,0:T(1,128)S(1)} async-done(((f32[32,2,1]{1,2,0:T(1,128)}), f32[32,2,1]{1,2,0:T(1,128)S(1)}, u32[]{:S(2)}, u32[]{:S(2)}) %all-to-all-start.2) | async-done | bytes 288 | tf_op jit(solution)/shard_map/all_to_all | solution.py:19
  161.2 0.6 fusion.18
  (33 shorter events, 1.7 us)
Async XLA Ops:
  7.2 9.0 %copy-start = (bf16[2048,32]{0,1:T(8,128)(2,1)S(1)}, bf16[2048,32]{0,1:T(8,128)(2,1)}, u32[]{:S(2)}) copy-start(bf16[2048,32]{0,1:T(8,128)(2,1)} %param.18) | copy-start | bytes 393220
  7.2 85.0 %all-gather.2.cloned.1.call-start = ((), (), s32[]{:S(2)}) async-start(), calls=%async_computation.3 | async-start | bytes 13369344 | tf_op jit(solution)/shard_map/all_gather | solution.py:84
  16.2 84.9 %copy-start.1 = (f32[2,1536,2]{1,2,0:T(2,128)S(1)}, f32[2,1536,2]{1,2,0:T(2,128)}, u32[]{:S(2)}) copy-start(f32[2,1536,2]{1,2,0:T(2,128)} %param.23) | copy-start | bytes 73732
  16.2 84.8 %copy-start.2 = (f32[2]{0:T(128)S(1)}, f32[2]{0:T(128)}, u32[]{:S(2)}) copy-start(f32[2]{0:T(128)} %param.21) | copy-start | bytes 28
  16.2 84.8 %copy-start.3 = (f32[2]{0:T(128)S(1)}, f32[2]{0:T(128)}, u32[]{:S(2)}) copy-start(f32[2]{0:T(128)} %param.22) | copy-start | bytes 28
  103.1 23.8 %collective-permute-start = (bf16[2,3,256]{1,2,0:T(8,128)(2,1)}, bf16[2,3,256]{1,2,0:T(8,128)(2,1)S(1)}, u32[]{:S(2)}, u32[]{:S(2)}) collective-permute-start(bf16[2,3,256]{1,2,0:T(8,128)(2,1)} %slice.58), channel_id=1, source_target_pairs={{0,16},{16,32},{32,48},{48,64},{64,80},{80,96},{96,112},{112,128},... | collective-permute-start | bytes 9224 | tf_op jit(solution)/shard_map/ppermute | solution.py:14
  107.1 19.7 %all-to-all-start = ((f32[2,1,2,32]{2,0,1,3:T(2,128)}), f32[2,1,2,32]{2,0,1,3:T(2,128)S(1)}, u32[]{:S(2)}, u32[]{:S(2)}) async-start(f32[2,1,2,32]{2,0,1,3:T(2,128)} %broadcast_in_dim.4), calls=%async_computation | async-start | bytes 65536 | tf_op jit(solution)/shard_map/all_to_all | solution.py:104
  129.5 17.1 %copy-start.4 = (bf16[2,128]{1,0:T(2,128)(2,1)S(1)}, bf16[2,128]{1,0:T(2,128)(2,1)}, u32[]{:S(2)}) copy-start(bf16[2,128]{1,0:T(2,128)(2,1)} %param.26) | copy-start | bytes 1540
  132.1 14.4 %all-to-all-start.1 = ((f32[2,1,2,64,128]{4,2,0,1,3:T(2,128)}), f32[2,1,2,64,128]{4,2,0,1,3:T(2,128)S(1)}, u32[]{:S(2)}, u32[]{:S(2)}) async-start(f32[2,1,2,64,128]{4,2,0,1,3:T(2,128)} %copy.30), calls=%async_computation.1 | async-start | bytes 262144 | tf_op jit(solution)/shard_map/all_to_all | solution.py:103
  147.7 13.5 %all-to-all-start.2 = ((f32[32,2,1]{1,2,0:T(1,128)}), f32[32,2,1]{1,2,0:T(1,128)S(1)}, u32[]{:S(2)}, u32[]{:S(2)}) async-start(f32[32,2,1]{1,2,0:T(1,128)} %broadcast_in_dim.5), calls=%async_computation.2 | async-start | bytes 32768 | tf_op jit(solution)/shard_map/all_to_all | solution.py:19
Sparse Core Ops, SparseCore 0:
  10.1 82.0 all-gather.1
where the time goes:
time: 169 us
  waiting for transfers between devices  105 us (62%)
  starting transfers between devices  21 us (12%)
  between operations  14.2 us (8%)
  matrix products  10.2 us (6%)
  other arithmetic  9.05 us (5%)
  local copies, waits for them, and re-layouts  8.84 us (5%)
    all_gather x1, waiting for transfers between devices, per_device(): lax.all_gather(hidden_in, 'tp', axis=1, tiled=True)  75.9 us
    all_to_all x1, waiting for transfers between devices, per_device(): lax.all_to_all(seg_states[:, None], 'sp', split_axis=3, concat_axis=1, ti...  10.3 us
    all_to_all x1, starting transfers between devices, per_device(): lax.all_to_all(tiled_totals, 'sp', split_axis=3, concat_axis=1, tiled=True)  9.89 us
    all_to_all x1, waiting for transfers between devices, per_device(): lax.all_to_all(tiled_totals, 'sp', split_axis=3, concat_axis=1, tiled=True)  9.54 us
    all_to_all x1, waiting for transfers between devices, sent_to_all(): lax.all_to_all(jnp.broadcast_to(shard[None], (length, *shard.shape)), axi...  8.94 us
    dot_general x1, matrix products, per_device(): jnp.einsum('tfy,yz->tfz', lax.all_gather(hidden_in, 'tp', axis=1, tiled=T...  8.12 us
    all_to_all x1, starting transfers between devices, per_device(): lax.all_to_all(seg_states[:, None], 'sp', split_axis=3, concat_axis=1, ti...  3.85 us
    all_to_all x1, starting transfers between devices, sent_to_all(): lax.all_to_all(jnp.broadcast_to(shard[None], (length, *shard.shape)), axi...  3.85 us
  transfers between devices with their start and end apart: 5, of which 4 were waited for; matrix products, arithmetic and copies ran while one was open for 6% of the time, Pallas kernels for 0%

commit v1 on v0

--- a/solution.py
+++ b/solution.py
@@ -81,7 +81,9 @@
     w_joined = jnp.concatenate([w_value, w_key, own_step], axis=1)
     projected = jnp.einsum(
         "tfy,yz->tfz",
-        lax.all_gather(hidden_in, "tp", axis=1, tiled=True),
+        jnp.concatenate(
+            lax.all_to_all(jnp.stack([hidden_in] * lax.axis_size("tp")), "tp", 0, 0), axis=1
+        ),
         w_joined,
         preferred_element_type=jnp.float32,
     ).astype(jnp.bfloat16)

time: 169 us -> 372 us (2.20)
  waiting for transfers between devices: 105 us -> 295 us
  starting transfers between devices: 21 us -> 36 us
  local copies, waits for them, and re-layouts: 8.84 us -> 22.2 us
  between operations: 14.2 us -> 0.94 us
    all_to_all x0 -> x1, waiting for transfers between devices: none -> 272 us  [per_device(): lax.all_to_all(jnp.stack([hidden_in] * lax.axis_size('tp')), 'tp', 0, 0)]
    all_gather x1 -> x0, waiting for transfers between devices: 75.9 us -> none  [per_device(): lax.all_gather(hidden_in, 'tp', axis=1, tiled=True)]
    reshape x1 -> x2, local copies, waits for them, and re-layouts: 0.02 us -> 10.7 us  [the longest x1 10.7 us: per_device(): jnp.concatenate(lax.all_to_all(jnp.stack([hidden_in] * lax.axis_size('tp'...]
    all_to_all x0 -> x1, starting transfers between devices: none -> 10.4 us  [per_device(): lax.all_to_all(jnp.stack([hidden_in] * lax.axis_size('tp')), 'tp', 0, 0)]
    another operation x1 -> x2, local copies, waits for them, and re-layouts: 0.02 us -> 7.27 us  [the longest x1 7.25 us: per_device(): jnp.stack([hidden_in] * lax.axis_size('tp'))]
    all_to_all x1, waiting for transfers between devices: 9.54 us -> 4 us  [per_device(): lax.all_to_all(tiled_totals, 'sp', split_axis=3, concat_axis=1, tiled=True)]
    all_to_all x1, starting transfers between devices: 3.85 us -> 7.87 us  [per_device(): lax.all_to_all(seg_states[:, None], 'sp', split_axis=3, concat_axis=1, ti...]
  transfers between devices with their start and end apart: 5 -> 5, of which waited for: 4 -> 4; matrix products, arithmetic and copies ran while one was open for 6% -> 1% of each run, Pallas kernels for 0% -> 0%
where the time goes in v1:
time: 372 us
  waiting for transfers between devices  295 us (79%)
  starting transfers between devices  36 us (10%)
  local copies, waits for them, and re-layouts  22.2 us (6%)
  matrix products  10.2 us (3%)
  other arithmetic  6.9 us (2%)
    all_to_all x1, waiting for transfers between devices, per_device(): lax.all_to_all(jnp.stack([hidden_in] * lax.axis_size('tp')), 'tp', 0, 0)  272 us
    reshape x1, local copies, waits for them, and re-layouts, per_device(): jnp.concatenate(lax.all_to_all(jnp.stack([hidden_in] * lax.axis_size('tp'...  10.7 us
    all_to_all x1, starting transfers between devices, per_device(): lax.all_to_all(jnp.stack([hidden_in] * lax.axis_size('tp')), 'tp', 0, 0)  10.4 us
    all_to_all x1, waiting for transfers between devices, per_device(): lax.all_to_all(seg_states[:, None], 'sp', split_axis=3, concat_axis=1, ti...  10.3 us
    all_to_all x1, starting transfers between devices, per_device(): lax.all_to_all(tiled_totals, 'sp', split_axis=3, concat_axis=1, tiled=True)  10.2 us
    all_to_all x1, waiting for transfers between devices, sent_to_all(): lax.all_to_all(jnp.broadcast_to(shard[None], (length, *shard.shape)), axi...  8.94 us
    dot_general x1, matrix products, per_device(): jnp.einsum('tfy,yz->tfz', jnp.concatenate(lax.all_to_all(jnp.stack([hidde...  8.13 us
    all_to_all x1, starting transfers between devices, per_device(): lax.all_to_all(seg_states[:, None], 'sp', split_axis=3, concat_axis=1, ti...  7.87 us
  transfers between devices with their start and end apart: 5, of which 4 were waited for; matrix products, arithmetic and copies ran while one was open for 1% of the time, Pallas kernels for 0%

profile of v1, /device:TPU:24, one launch (start us, length us, event | category | flops | bytes accessed | tf_op | source)
XLA Modules:
  0.0 371.5 jit_solution(16428580625698088242)
XLA Ops:
  0.6 7.3 %stack.2 = bf16[16,2,96,2048]{3,2,1,0:T(8,128)(2,1)} broadcast(bf16[2,96,2048]{2,1,0:T(8,128)(2,1)} %param.15), dimensions={1,2,3} | broadcast | bytes 13369344 | tf_op jit(solution)/shard_map/stack | solution.py:85
  8.0 10.4 %all-to-all-start = ((bf16[16,2,96,2048]{3,2,1,0:T(8,128)(2,1)}), bf16[16,2,96,2048]{3,2,1,0:T(8,128)(2,1)}, u32[]{:S(2)}, u32[]{:S(2)}) async-start(bf16[16,2,96,2048]{3,2,1,0:T(8,128)(2,1)} %stack.2), calls=%async_computation | async-start | bytes 25165824 | tf_op jit(solution)/shard_map/all_to_all | solution.py:85
  18.4 0.2 copy.26
  18.7 0.2 copy.25
  19.2 0.6 multiply_reduce_fusion.1
  19.9 272.0 %all-to-all-done = bf16[16,2,96,2048]{3,2,1,0:T(8,128)(2,1)} async-done(((bf16[16,2,96,2048]{3,2,1,0:T(8,128)(2,1)}), bf16[16,2,96,2048]{3,2,1,0:T(8,128)(2,1)}, u32[]{:S(2)}, u32[]{:S(2)}) %all-to-all-start) | async-done | bytes 12582944 | tf_op jit(solution)/shard_map/all_to_all | solution.py:85
  292.0 10.7 %copy.27 = bf16[2,16,96,2048]{3,2,1,0:T(8,128)(2,1)} copy(bf16[2,16,96,2048]{3,2,0,1:T(8,128)(2,1)} %bitcast.1) | data formatting | bytes 25165824 | tf_op jit(solution)/shard_map/reshape | solution.py:84
  302.7 8.1 %fusion = bf16[2,1536,258]{1,2,0:T(8,128)(2,1)S(1)} fusion(bf16[2,1536,2048]{2,1,0:T(8,128)(2,1)} %bitcast.55, bf16[2048,2]{0,1:T(2,128)(2,1)S(1)} %constant_dynamic-slice_fusion, bf16[2048,128]{0,1:T(8,128)(2,1)S(1)} %copy.26, bf16[2048,128]{0,1:T(8,128)(2,1)S(1)} %copy.25), kind=kOutput, calls=%fused_computation.2 | convolution fusion | flops 3250354176 | bytes 15224832 | tf_op jit(solution)/shard_map/tfy,yz->tfz/dot_general | solution.py:82
  310.8 0.8 slice.58
  311.6 0.2 fusion.23
  311.8 0.6 broadcast_in_dim.4
  312.4 10.2 %all-to-all-start.1 = ((f32[2,1,2,32]{2,0,1,3:T(2,128)}), f32[2,1,2,32]{2,0,1,3:T(2,128)S(1)}, u32[]{:S(2)}, u32[]{:S(2)}) async-start(f32[2,1,2,32]{2,0,1,3:T(2,128)} %broadcast_in_dim.4), calls=%async_computation.1 | async-start | bytes 65536 | tf_op jit(solution)/shard_map/all_to_all | solution.py:106
  322.7 3.7 collective-permute-start
  326.4 1.2 reduce-window.6
  327.6 0.2 slice_reduce_fusion
  327.7 0.4 reduce-window.9
  328.2 0.1 bitcast_multiply_fusion
  328.5 4.0 %all-to-all-done.1 = f32[2,1,2,32]{2,0,1,3:T(2,128)S(1)} async-done(((f32[2,1,2,32]{2,0,1,3:T(2,128)}), f32[2,1,2,32]{2,0,1,3:T(2,128)S(1)}, u32[]{:S(2)}, u32[]{:S(2)}) %all-to-all-start.1) | async-done | bytes 544 | tf_op jit(solution)/shard_map/all_to_all | solution.py:106
  332.6 2.6 divide_multiply_fusion
  335.2 0.1 slice.68
  335.3 1.7 fusion.5
  337.0 0.7 copy.31
  337.7 7.9 %all-to-all-start.2 = ((f32[2,1,2,64,128]{4,2,0,1,3:T(2,128)}), f32[2,1,2,64,128]{4,2,0,1,3:T(2,128)S(1)}, u32[]{:S(2)}, u32[]{:S(2)}) async-start(f32[2,1,2,64,128]{4,2,0,1,3:T(2,128)} %copy.31), calls=%async_computation.2 | async-start | bytes 262144 | tf_op jit(solution)/shard_map/all_to_all | solution.py:105
  345.8 10.3 %all-to-all-done.2 = f32[2,1,2,64,128]{4,2,0,1,3:T(2,128)S(1)} async-done(((f32[2,1,2,64,128]{4,2,0,1,3:T(2,128)}), f32[2,1,2,64,128]{4,2,0,1,3:T(2,128)S(1)}, u32[]{:S(2)}, u32[]{:S(2)}) %all-to-all-start.2) | async-done | bytes 131104 | tf_op jit(solution)/shard_map/all_to_all | solution.py:105
  356.1 0.2 fusion.13
  356.3 0.2 fusion.19
  356.5 0.2 multiply_reduce_fusion
  356.7 0.6 broadcast_in_dim.5
  357.3 3.8 %all-to-all-start.3 = ((f32[32,2,1]{1,2,0:T(1,128)}), f32[32,2,1]{1,2,0:T(1,128)S(1)}, u32[]{:S(2)}, u32[]{:S(2)}) async-start(f32[32,2,1]{1,2,0:T(1,128)} %broadcast_in_dim.5), calls=%async_computation.3 | async-start | bytes 32768 | tf_op jit(solution)/shard_map/all_to_all | solution.py:19
  361.3 0.6 convert_element_type.93
  361.9 8.9 %all-to-all-done.3 = f32[32,2,1]{1,2,0:T(1,128)S(1)} async-done(((f32[32,2,1]{1,2,0:T(1,128)}), f32[32,2,1]{1,2,0:T(1,128)S(1)}, u32[]{:S(2)}, u32[]{:S(2)}) %all-to-all-start.3) | async-done | bytes 288 | tf_op jit(solution)/shard_map/all_to_all | solution.py:19
  370.9 0.6 fusion.18
  (56 shorter events, 1.1 us)
Async XLA Ops:
  0.6 19.3 %copy-start = (bf16[2048,32]{0,1:T(8,128)(2,1)S(1)}, bf16[2048,32]{0,1:T(8,128)(2,1)}, u32[]{:S(2)}) copy-start(bf16[2048,32]{0,1:T(8,128)(2,1)} %param.18) | copy-start | bytes 393220
  7.9 10.5 %copy-start.1 = (bf16[2048,128]{1,0:T(8,128)(2,1)S(1)}, bf16[2048,128]{1,0:T(8,128)(2,1)}, u32[]{:S(2)}) copy-start(bf16[2048,128]{1,0:T(8,128)(2,1)} %param.17) | copy-start | bytes 1572868
  7.9 10.8 %copy-start.2 = (bf16[2048,128]{1,0:T(8,128)(2,1)S(1)}, bf16[2048,128]{1,0:T(8,128)(2,1)}, u32[]{:S(2)}) copy-start(bf16[2048,128]{1,0:T(8,128)(2,1)} %param.16) | copy-start | bytes 1572868
  7.9 11.0 %copy-start.11 = (bf16[128]{0:T(256)(128)(2,1)S(1)}, bf16[128]{0:T(256)(128)(2,1)}, u32[]{:S(2)}) copy-start(bf16[128]{0:T(256)(128)(2,1)} %param.29) | copy-start | bytes 772
  7.9 11.1 %copy-start.12 = (bf16[2,128]{1,0:T(2,128)(2,1)S(1)}, bf16[2,128]{1,0:T(2,128)(2,1)}, u32[]{:S(2)}) copy-start(bf16[2,128]{1,0:T(2,128)(2,1)} %param.27) | copy-start | bytes 1540
  7.9 11.2 %copy-start.9 = (bf16[2,128]{1,0:T(2,128)(2,1)S(1)}, bf16[2,128]{1,0:T(2,128)(2,1)}, u32[]{:S(2)}) copy-start(bf16[2,128]{1,0:T(2,128)(2,1)} %param.24) | copy-start | bytes 1540
  7.9 11.2 %copy-start.8 = (f32[2]{0:T(128)S(1)}, f32[2]{0:T(128)}, u32[]{:S(2)}) copy-start(f32[2]{0:T(128)} %param.22) | copy-start | bytes 28
  7.9 11.2 %copy-start.5 = (bf16[4,128]{1,0:T(4,128)(2,1)S(1)}, bf16[4,128]{1,0:T(4,128)(2,1)}, u32[]{:S(2)}) copy-start(bf16[4,128]{1,0:T(4,128)(2,1)} %param.19) | copy-start | bytes 3076
  7.9 11.2 %copy-start.6 = (bf16[4,128]{1,0:T(4,128)(2,1)S(1)}, bf16[4,128]{1,0:T(4,128)(2,1)}, u32[]{:S(2)}) copy-start(bf16[4,128]{1,0:T(4,128)(2,1)} %param.20) | copy-start | bytes 3076
  8.0 11.3 %copy-start.13 = (bf16[2,128]{1,0:T(2,128)(2,1)S(1)}, bf16[2,128]{1,0:T(2,128)(2,1)}, u32[]{:S(2)}) copy-start(bf16[2,128]{1,0:T(2,128)(2,1)} %param.25) | copy-start | bytes 1540
  8.0 11.2 %copy-start.14 = (bf16[2,128]{1,0:T(2,128)(2,1)S(1)}, bf16[2,128]{1,0:T(2,128)(2,1)}, u32[]{:S(2)}) copy-start(bf16[2,128]{1,0:T(2,128)(2,1)} %param.26) | copy-start | bytes 1540
  8.0 11.9 %copy-start.4 = (f32[2]{0:T(128)S(1)}, f32[2]{0:T(128)}, u32[]{:S(2)}) copy-start(f32[2]{0:T(128)} %param.21) | copy-start | bytes 28
  8.0 11.9 %copy-start.7 = (f32[2,2]{1,0:T(2,128)S(1)}, f32[2,2]{1,0:T(2,128)}, u32[]{:S(2)}) copy-start(f32[2,2]{1,0:T(2,128)} %param.28) | copy-start | bytes 52
  8.0 284.0 %all-to-all-start = ((bf16[16,2,96,2048]{3,2,1,0:T(8,128)(2,1)}), bf16[16,2,96,2048]{3,2,1,0:T(8,128)(2,1)}, u32[]{:S(2)}, u32[]{:S(2)}) async-start(bf16[16,2,96,2048]{3,2,1,0:T(8,128)(2,1)} %stack.2), calls=%async_computation | async-start | bytes 25165824 | tf_op jit(solution)/shard_map/all_to_all | solution.py:85
  302.7 8.9 %copy-start.3 = (f32[2,1536,2]{1,2,0:T(2,128)S(1)}, f32[2,1536,2]{1,2,0:T(2,128)}, u32[]{:S(2)}) copy-start(f32[2,1536,2]{1,2,0:T(2,128)} %param.23) | copy-start | bytes 73732
  312.4 20.0 %all-to-all-start.1 = ((f32[2,1,2,32]{2,0,1,3:T(2,128)}), f32[2,1,2,32]{2,0,1,3:T(2,128)S(1)}, u32[]{:S(2)}, u32[]{:S(2)}) async-start(f32[2,1,2,32]{2,0,1,3:T(2,128)} %broadcast_in_dim.4), calls=%async_computation.1 | async-start | bytes 65536 | tf_op jit(solution)/shard_map/all_to_all | solution.py:106
  322.7 9.9 %collective-permute-start = (bf16[2,3,256]{1,2,0:T(8,128)(2,1)}, bf16[2,3,256]{1,2,0:T(8,128)(2,1)S(1)}, u32[]{:S(2)}, u32[]{:S(2)}) collective-permute-start(bf16[2,3,256]{1,2,0:T(8,128)(2,1)} %slice.58), channel_id=1, source_target_pairs={{0,16},{16,32},{32,48},{48,64},{64,80},{80,96},{96,112},{112,128},... | collective-permute-start | bytes 9224 | tf_op jit(solution)/shard_map/ppermute | solution.py:14
  335.2 21.2 %copy-start.15 = (bf16[2,128]{1,0:T(2,128)(2,1)S(1)}, bf16[2,128]{1,0:T(2,128)(2,1)}, u32[]{:S(2)}) copy-start(bf16[2,128]{1,0:T(2,128)(2,1)} %param.26) | copy-start | bytes 1540
  335.2 21.4 %copy-start.10 = (f32[2]{0:T(128)S(1)}, f32[2]{0:T(128)}, u32[]{:S(2)}) copy-start(f32[2]{0:T(128)} %multiply_reduce_fusion.1) | copy-start | bytes 28
  337.7 18.4 %all-to-all-start.2 = ((f32[2,1,2,64,128]{4,2,0,1,3:T(2,128)}), f32[2,1,2,64,128]{4,2,0,1,3:T(2,128)S(1)}, u32[]{:S(2)}, u32[]{:S(2)}) async-start(f32[2,1,2,64,128]{4,2,0,1,3:T(2,128)} %copy.31), calls=%async_computation.2 | async-start | bytes 262144 | tf_op jit(solution)/shard_map/all_to_all | solution.py:105
  357.3 13.4 %all-to-all-start.3 = ((f32[32,2,1]{1,2,0:T(1,128)}), f32[32,2,1]{1,2,0:T(1,128)S(1)}, u32[]{:S(2)}, u32[]{:S(2)}) async-start(f32[32,2,1]{1,2,0:T(1,128)} %broadcast_in_dim.5), calls=%async_computation.3 | async-start | bytes 32768 | tf_op jit(solution)/shard_map/all_to_all | solution.py:19
